TPU v7x, 32 devices: a whole 2x2x4 slice. The times are simulated.
32 devices in a mesh: sp: 8 (over z, y), dp: 4 (over x, core).
Axes of the slice: x: 2, y: 2, z: 4, core: 2. Of those that a mesh axis runs over, the one named last changes fastest.
Arguments:
- queries: bfloat16 [4, 1024, 16, 128], P('dp', 'sp'), may hold values from -7 to 7
- key_vectors: bfloat16 [4, 1024, 16, 128], P('dp', 'sp'), may hold values from -6 to 6
- value_vectors: bfloat16 [4, 1024, 16, 128], P('dp', 'sp'), may hold values from -6 to 6
- head_lambda: float32 [16], P('sp'), may hold values from 0.3 to 0.8
- head_gain: float32 [128], replicated, may hold values from 0.1 to 1.9
- residual: bfloat16 [4, 1024, 2048], P('dp', 'sp'), may hold values from -6 to 6
- out_weight: bfloat16 [2048, 2048], replicated, may hold values from -0.125 to 0.125
- mix_gain: float32 [2048], replicated, may hold values from 0.1 to 1.9
- pre_gain: float32 [2048], replicated, may hold values from 0.1 to 1.9
- post_gain: float32 [2048], replicated, may hold values from 0.1 to 1.9
- routes: int32 [4, 1024, 4], P('dp', 'sp'), may hold values from 0 to 31, all different within a row; in each aligned block of 128 rows (0 to 127, 128 to 255, ..., all dimensions but the last counted through in order) at most 24 rows name the same one
- route_weights: float32 [4, 1024, 4], P('dp', 'sp'), may hold values from 0.25 to 1
- expert_gate: bfloat16 [32, 2048, 512], P(('sp', 'dp')), may hold values from -0.125 to 0.125
- expert_up: bfloat16 [32, 2048, 512], P(('sp', 'dp')), may hold values from -0.125 to 0.125
- expert_down: bfloat16 [32, 512, 2048], P(('sp', 'dp')), may hold values from -0.25 to 0.25
- shared_gate: bfloat16 [2048, 512], replicated, may hold values from -0.125 to 0.125
- shared_up: bfloat16 [2048, 512], replicated, may hold values from -0.125 to 0.125
- shared_down: bfloat16 [512, 2048], replicated, may hold values from -0.25 to 0.25
Outputs:
- output: bfloat16 [4, 1024, 2048], P('dp', 'sp')
Inputs may be any that keep to these rules, and one draw needn't show every extreme that they name: `routes`: among the tokens of one device (aligned blocks of 128 positions), no expert is named more than 24 times; in some block some expert is named exactly 24 times. Each token names 4 different experts.
All inputs are finite; a program needn't handle non-finite values.
Results may differ from a plain program's by a relative error of at most 0.0075.
Values may be sent and summed in bfloat16 or wider, within the bound.
No kernel may reach another device: no remote copies, remote signals or barrier semaphores. Data moves between devices by JAX's collectives and lax.ppermute only.
A program may use at most 128 MiB of HBM per device.

v0:
```python
import jax
import jax.numpy as jnp
from jax import lax
from jax.sharding import PartitionSpec as P

epsilon = 1e-06


def rms_scale(values_in, gain):
    return (
        values_in
        * lax.rsqrt(jnp.mean(values_in * values_in, axis=-1, keepdims=True) + epsilon)
        * gain
    )


def feed_forward(rows, gate_w, up_w, down_w):
    gate_val = jnp.dot(rows, gate_w, preferred_element_type=jnp.float32)
    up_val = jnp.dot(rows, up_w, preferred_element_type=jnp.float32)
    hidden = (jax.nn.silu(gate_val) * up_val).astype(jnp.bfloat16)
    return jnp.dot(hidden, down_w, preferred_element_type=jnp.float32).astype(jnp.bfloat16)


def attend_heads(query_heads, key_heads, value_heads, head_lambda, head_gain):
    length = query_heads.shape[0]
    head_count = query_heads.shape[1]
    head_size = query_heads.shape[2] // 2
    block_rows = min(512, length)
    block_count = length // block_rows
    query_blocks = query_heads.reshape(block_count, block_rows, head_count, 2, head_size)
    key_all = key_heads.reshape(length, head_count, 2, head_size)
    key_pos = jnp.arange(length, dtype=jnp.int32)

    def one_block(inputs):
        query_block, block_index = inputs
        scores = jnp.einsum(
            "qhmd,khmd->hmqk", query_block, key_all, preferred_element_type=jnp.float32
        ) * head_size ** (-0.5)
        query_pos = block_index * block_rows + jnp.arange(block_rows, dtype=jnp.int32)
        causal = key_pos[None, :] <= query_pos[:, None]
        scores = jnp.where(causal, scores, -jnp.inf)
        maxima = jnp.max(scores, axis=-1, keepdims=True)
        exponent = jnp.exp(scores - maxima)
        softmax_both = exponent / jnp.sum(exponent, axis=-1, keepdims=True)
        mixture = (softmax_both[:, 0] - head_lambda[:, None, None] * softmax_both[:, 1]).astype(
            jnp.bfloat16
        )
        head_output = jnp.einsum(
            "hqk,khe->qhe", mixture, value_heads, preferred_element_type=jnp.float32
        )
        return rms_scale(head_output, head_gain).astype(jnp.bfloat16)

    outputs = lax.map(one_block, (query_blocks, jnp.arange(block_count, dtype=jnp.int32)))
    return outputs.reshape(length, head_count, -1)


def local(
    queries,
    key_vectors,
    value_vectors,
    head_lambda,
    head_gain,
    residual,
    out_weight,
    mix_gain,
    pre_gain,
    post_gain,
    routes,
    route_weights,
    expert_gate,
    expert_up,
    expert_down,
    shared_gate,
    shared_up,
    shared_down,
):
    query_heads, key_heads, value_heads = (
        lax.all_to_all(queries[0], "sp", split_axis=1, concat_axis=0, tiled=True),
        lax.all_to_all(key_vectors[0], "sp", split_axis=1, concat_axis=0, tiled=True),
        lax.all_to_all(value_vectors[0], "sp", split_axis=1, concat_axis=0, tiled=True),
    )
    attended = attend_heads(query_heads, key_heads, value_heads, head_lambda, head_gain)
    token_heads = lax.all_to_all(attended, "sp", split_axis=0, concat_axis=1, tiled=True)
    tok_count = token_heads.shape[0]
    flat_heads = token_heads.reshape(tok_count, -1)
    mixed_rows = jnp.dot(flat_heads, out_weight, preferred_element_type=jnp.float32)
    updated = (residual[0].astype(jnp.float32) + rms_scale(mixed_rows, mix_gain)).astype(
        jnp.bfloat16
    )
    normed = rms_scale(updated.astype(jnp.float32), pre_gain).astype(jnp.bfloat16)
    model_width = normed.shape[1]
    experts_total = lax.axis_size("sp") * lax.axis_size("dp")
    top_count = routes.shape[2]
    capacity = 3 * tok_count * top_count // (2 * experts_total)
    assign_count = tok_count * top_count
    flat_routes = routes[0].reshape(assign_count)
    one_hot = (flat_routes[:, None] == jnp.arange(experts_total, dtype=jnp.int32)[None, :]).astype(
        jnp.int32
    )
    earlier = jnp.cumsum(one_hot, axis=0) - one_hot
    rank_index = jnp.sum(earlier * one_hot, axis=1)
    slot_index = flat_routes * capacity + rank_index
    source_row = (
        jnp.zeros((experts_total * capacity,), jnp.int32)
        .at[slot_index]
        .set(jnp.arange(assign_count, dtype=jnp.int32) // top_count)
    )
    occupied = (
        jnp.zeros((experts_total * capacity,), jnp.bfloat16)
        .at[slot_index]
        .set(jnp.ones((assign_count,), jnp.bfloat16))
    )
    outgoing = (normed[source_row] * occupied[:, None]).reshape(
        experts_total, capacity, model_width
    )
    shared_out = feed_forward(normed, shared_gate, shared_up, shared_down)
    arrived = lax.all_to_all(outgoing, ("sp", "dp"), split_axis=0, concat_axis=0, tiled=True)
    flat_rows = arrived.reshape(-1, model_width)
    result_rows = feed_forward(flat_rows, expert_gate[0], expert_up[0], expert_down[0])
    results = result_rows.reshape(arrived.shape[0], -1, model_width)
    returned = lax.all_to_all(results, ("sp", "dp"), split_axis=0, concat_axis=0, tiled=True)
    picked = returned.reshape(experts_total * capacity, model_width)[slot_index]
    routed = jnp.sum(
        picked.astype(jnp.float32).reshape(tok_count, top_count, model_width)
        * route_weights[0][:, :, None],
        axis=1,
    )
    combined = routed + shared_out.astype(jnp.float32)
    output = (updated.astype(jnp.float32) + rms_scale(combined, post_gain)).astype(jnp.bfloat16)
    return output.reshape(1, tok_count, model_width)


def solution(mesh):
    in_specs = (
        P("dp", "sp", None, None),
        P("dp", "sp", None, None),
        P("dp", "sp", None, None),
        P("sp"),
        P(),
        P("dp", "sp", None),
        P(),
        P(),
        P(),
        P(),
        P("dp", "sp", None),
        P("dp", "sp", None),
        P(("sp", "dp"), None, None),
        P(("sp", "dp"), None, None),
        P(("sp", "dp"), None, None),
        P(),
        P(),
        P(),
    )
    out_specs = P("dp", "sp", None)
    return jax.shard_map(local, mesh=mesh, in_specs=in_specs, out_specs=out_specs, check_vma=False)
```

profile of v0, /device:TPU:0, one launch (start us, length us, event | category | flops | bytes accessed | tf_op | source)
XLA Modules:
  0.0 313.4 jit_solution(17790925592510892741)
XLA Ops:
  2.1 7.3 %all-to-all-start = ((bf16[128,16,128]{2,0,1:T(8,128)(2,1)}), bf16[128,16,128]{2,0,1:T(8,128)(2,1)S(1)}, u32[]{:S(2)}, u32[]{:S(2)}) async-start(bf16[128,16,128]{2,0,1:T(8,128)(2,1)} %bitcast.132), calls=%async_computation | async-start | bytes 1048576 | tf_op jit(solution)/shard_map/all_to_all | solution.py:78
  11.4 12.5 %all-to-all-done = bf16[128,16,128]{2,0,1:T(8,128)(2,1)S(1)} async-done(((bf16[128,16,128]{2,0,1:T(8,128)(2,1)}), bf16[128,16,128]{2,0,1:T(8,128)(2,1)S(1)}, u32[]{:S(2)}, u32[]{:S(2)}) %all-to-all-start) | async-done | bytes 524320 | tf_op jit(solution)/shard_map/all_to_all | solution.py:78
  23.9 3.6 %all-to-all-start.2 = ((bf16[128,16,128]{2,0,1:T(8,128)(2,1)}), bf16[128,16,128]{2,0,1:T(8,128)(2,1)S(1)}, u32[]{:S(2)}, u32[]{:S(2)}) async-start(bf16[128,16,128]{2,0,1:T(8,128)(2,1)} %bitcast.155), calls=%async_computation.2 | async-start | bytes 1048576 | tf_op jit(solution)/shard_map/all_to_all | solution.py:80
  29.5 12.7 %all-to-all-done.2 = bf16[128,16,128]{2,0,1:T(8,128)(2,1)S(1)} async-done(((bf16[128,16,128]{2,0,1:T(8,128)(2,1)}), bf16[128,16,128]{2,0,1:T(8,128)(2,1)S(1)}, u32[]{:S(2)}, u32[]{:S(2)}) %all-to-all-start.2) | async-done | bytes 524320 | tf_op jit(solution)/shard_map/all_to_all | solution.py:80
  42.2 4.1 %all-to-all-start.1 = ((bf16[128,16,128]{2,0,1:T(8,128)(2,1)}), bf16[128,16,128]{2,0,1:T(8,128)(2,1)}, u32[]{:S(2)}, u32[]{:S(2)}) async-start(bf16[128,16,128]{2,0,1:T(8,128)(2,1)} %bitcast.154), calls=%async_computation.1 | async-start | bytes 1048576 | tf_op jit(solution)/shard_map/all_to_all | solution.py:79
  52.8 7.8 %all-to-all-done.1 = bf16[128,16,128]{2,0,1:T(8,128)(2,1)} async-done(((bf16[128,16,128]{2,0,1:T(8,128)(2,1)}), bf16[128,16,128]{2,0,1:T(8,128)(2,1)}, u32[]{:S(2)}, u32[]{:S(2)}) %all-to-all-start.1) | async-done | bytes 524320 | tf_op jit(solution)/shard_map/all_to_all | solution.py:79
  63.1 29.6 %while.11 = (s32[]{:T(128)}, bf16[2,512,2,128]{3,1,0,2:T(8,128)(2,1)}, s32[2]{0:T(128)S(1)}, bf16[2,512,2,2,64]{1,4,3,2,0:T(8,128)(2,1)S(1)}, bf16[1024,2,2,64]{...) while((s32[]{:T(128)}, ...), condition=%wide.region_4.5_spmd.clone, body=%wide.region_0.4_spmd.clone.sunk | while | flops 551684608 | bytes 40408232 | solution.py:53
  64.9 7.1 %fusion.99 = (f32[2,2,512]{2,1,0:T(2,128)S(1)}, f32[2,2,512,1024]{3,2,1,0:T(8,128)}) fusion(pred[512,1024]{1,0:T(8,128)(4,1)S(1)} %iota_compare_fusion.4, bf16[1024,2,2,64]{0,3,2,1:T(8,128)(2,1)} %get-tuple-element.202, bf16[2,512,2,2,64]{1,4,3,2,0:T(8,128)(2,1)S(1)} %get-tuple-element.201, s32[]{:T(128)} %get-tuple-element.188), kind=kOutput, calls=%fused_computation.102.clone.1 | convolution fusion | flops 276825088 | bytes 9707524 | tf_op jit(solution)/shard_map/while/body/eval_jaxpr/sub | solution.py:43
  72.0 4.0 %broadcast_divide_fusion.2 = f32[2,2,512,1024]{3,2,1,0:T(8,128)S(1)} fusion(f32[2,2,512,1024]{3,2,1,0:T(8,128)} %get-tuple-element.174, f32[2,2,512]{2,1,0:T(2,128)S(1)} %get-tuple-element.175), kind=kLoop, calls=%fused_computation.14.clone.1 | loop fusion | flops 2097152 | bytes 16785408 | tf_op jit(solution)/shard_map/while/body/eval_jaxpr/div | solution.py:44
  79.7 7.1 %fusion.99 = (f32[2,2,512]{2,1,0:T(2,128)S(1)}, f32[2,2,512,1024]{3,2,1,0:T(8,128)}) fusion(pred[512,1024]{1,0:T(8,128)(4,1)S(1)} %iota_compare_fusion.4, bf16[1024,2,2,64]{0,3,2,1:T(8,128)(2,1)} %get-tuple-element.202, bf16[2,512,2,2,64]{1,4,3,2,0:T(8,128)(2,1)S(1)} %get-tuple-element.201, s32[]{:T(128)} %get-tuple-element.188), kind=kOutput, calls=%fused_computation.102.clone.1 | convolution fusion | flops 276825088 | bytes 9707524 | tf_op jit(solution)/shard_map/while/body/eval_jaxpr/sub | solution.py:43
  86.8 4.0 %broadcast_divide_fusion.2 = f32[2,2,512,1024]{3,2,1,0:T(8,128)S(1)} fusion(f32[2,2,512,1024]{3,2,1,0:T(8,128)} %get-tuple-element.174, f32[2,2,512]{2,1,0:T(2,128)S(1)} %get-tuple-element.175), kind=kLoop, calls=%fused_computation.14.clone.1 | loop fusion | flops 2097152 | bytes 16785408 | tf_op jit(solution)/shard_map/while/body/eval_jaxpr/div | solution.py:44
  95.1 3.6 %all-to-all-start.3 = ((bf16[1024,2,128]{2,1,0:T(2,128)(2,1)}), bf16[1024,2,128]{2,1,0:T(2,128)(2,1)S(1)}, u32[]{:S(2)}, u32[]{:S(2)}) async-start(bf16[1024,2,128]{2,1,0:T(2,128)(2,1)} %copy.59), calls=%async_computation.3 | async-start | bytes 1048576 | tf_op jit(solution)/shard_map/all_to_all | solution.py:83
  101.7 3.8 %scatter_custom_fusion.1 = bf16[768]{0:T(1024)(128)(2,1)S(1)} fusion(s32[512]{0:T(512)S(1)} %bitcast.160, bf16[512]{0:T(512)(128)(2,1)S(1)} %broadcast.140, bf16[]{:T(256)} %constant.60.clone.1), kind=kCustom, calls=%fused_computation.94 | custom fusion | bytes 1538 | tf_op jit(solution)/shard_map/scatter | solution.py:111
  105.6 7.6 %all-to-all-done.3 = bf16[1024,2,128]{2,1,0:T(2,128)(2,1)S(1)} async-done(((bf16[1024,2,128]{2,1,0:T(2,128)(2,1)}), bf16[1024,2,128]{2,1,0:T(2,128)(2,1)S(1)}, u32[]{:S(2)}, u32[]{:S(2)}) %all-to-all-start.3) | async-done | bytes 524320 | tf_op jit(solution)/shard_map/all_to_all | solution.py:83
  113.7 4.8 %multiply_reduce_fusion.3 = (f32[128]{0:T(128)S(1)}, f32[128,2048]{1,0:T(8,128)S(1)}) fusion(bf16[128,2048]{0,1:T(8,128)(2,1)S(1)} %bitcast.148, bf16[2048,2048]{1,0:T(8,128)(2,1)} %param.26), kind=kOutput, calls=%fused_computation.61 | convolution fusion | flops 1074265984 | bytes 9961984 | tf_op jit(solution)/shard_map/dot_general | solution.py:86
  119.1 4.3 %gather_fusion = bf16[768,2048]{1,0:T(8,128)(2,1)} fusion(bf16[128,2048]{1,0:T(8,128)(2,1)S(1)} %fusion.47, s32[1024]{0:T(1024)S(1)} %pad_clamp_fusion.1), kind=kCustom, calls=%fused_computation | custom fusion | bytes 6294528 | tf_op jit(solution)/shard_map/gather | solution.py:113
  125.5 74.6 %all_to_all.73 = bf16[32,24,2048]{2,1,0:T(8,128)(2,1)S(1)} all-to-all(bf16[32,24,2048]{2,1,0:T(8,128)(2,1)S(1)} %broadcast_multiply_fusion), channel_id=1, replica_groups=mesh['sp'=8,'dp'=4] {'sp','dp'}, dimensions={0} | all-to-all | bytes 6291456 | tf_op jit(solution)/shard_map/all_to_all | solution.py:117
  204.8 8.1 %convolution_convert_fusion = bf16[768,2048]{1,0:T(8,128)(2,1)} fusion(bf16[1,512,2048]{2,1,0:T(8,128)(2,1)S(1)} %copy-done, f32[768,512]{1,0:T(8,128)} %fusion.40, bf16[768,2048]{1,0:T(8,128)(2,1)} %bitcast.151, bf16[1,2048,512]{2,1,0:T(8,128)(2,1)} %param.33), kind=kOutput, calls=%fused_computation.38 | convolution fusion | flops 3225157632 | bytes 12058624 | tf_op jit(solution)/shard_map/dot_general | solution.py:21
  212.9 4.0 %all-to-all-start.5 = ((bf16[32,24,2048]{2,1,0:T(8,128)(2,1)}), bf16[32,24,2048]{2,1,0:T(8,128)(2,1)}, u32[]{:S(2)}, u32[]{:S(2)}) async-start(bf16[32,24,2048]{2,1,0:T(8,128)(2,1)} %bitcast.149), calls=%async_computation.5 | async-start | bytes 6291456 | tf_op jit(solution)/shard_map/all_to_all | solution.py:121
  219.1 69.1 %all-to-all-done.5 = bf16[32,24,2048]{2,1,0:T(8,128)(2,1)} async-done(((bf16[32,24,2048]{2,1,0:T(8,128)(2,1)}), bf16[32,24,2048]{2,1,0:T(8,128)(2,1)}, u32[]{:S(2)}, u32[]{:S(2)}) %all-to-all-start.5) | async-done | bytes 3145760 | tf_op jit(solution)/shard_map/all_to_all | solution.py:121
  288.2 7.5 %gather_fusion.1 = bf16[512,2048]{1,0:T(8,128)(2,1)} fusion(bf16[768,2048]{1,0:T(8,128)(2,1)} %bitcast.23, s32[1024]{0:T(1024)S(1)} %pad_clamp_fusion), kind=kCustom, calls=%fused_computation.1 | custom fusion | bytes 4196352 | tf_op jit(solution)/shard_map/gather | solution.py:122
  295.7 4.8 %reshape.143 = f32[128,4,2048]{2,1,0:T(4,128)} reshape(bf16[512,2048]{1,0:T(8,128)(2,1)} %gather_fusion.1) | data formatting | bytes 6291456 | tf_op jit(solution)/shard_map/convert_element_type | solution.py:124
  300.4 6.3 %multiply_reduce_fusion.1 = f32[128,2048]{1,0:T(8,128)} fusion(f32[128,4,2048]{2,1,0:T(4,128)} %reshape.143, f32[128,4]{1,0:T(8,128)S(1)} %copy.66), kind=kLoop, calls=%fused_computation.37 | loop fusion | flops 1835008 | bytes 5244928 | tf_op jit(solution)/shard_map/reduce_sum | solution.py:123
  306.8 4.3 %multiply_reduce_fusion.2 = (f32[128]{0:T(128)S(1)}, f32[128,2048]{1,0:T(8,128)}) fusion(f32[128,2048]{1,0:T(8,128)} %multiply_reduce_fusion.1, bf16[512,2048]{1,0:T(8,128)(2,1)} %param.37, bf16[128,2048]{1,0:T(8,128)(2,1)S(1)} %fusion.47, bf16[2048,512]{1,0:T(8,128)(2,1)} %param.36, f32[128,512]{1,0:T(8,128)S(1)} %fusion.78), kind=kOutput, calls=%fused_computation.60 | convolution fusion | flops 538574720 | bytes 7078400 | tf_op jit(solution)/shard_map/dot_general | solution.py:21
  (92 shorter events, 38.4 us)
Async XLA Ops:
  0.0 204.8 %copy-start = (bf16[1,512,2048]{2,1,0:T(8,128)(2,1)S(1)}, bf16[1,512,2048]{2,1,0:T(8,128)(2,1)}, u32[]{:S(2)}) copy-start(bf16[1,512,2048]{2,1,0:T(8,128)(2,1)} %param.34) | copy-start | bytes 6291460
  0.0 46.4 %copy-start.10 = (s32[1,128,4]{1,2,0:T(4,128)S(1)}, s32[1,128,4]{1,2,0:T(4,128)}, u32[]{:S(2)}) copy-start(s32[1,128,4]{1,2,0:T(4,128)} %param.30) | copy-start | bytes 6148
  2.1 21.8 %all-to-all-start = ((bf16[128,16,128]{2,0,1:T(8,128)(2,1)}), bf16[128,16,128]{2,0,1:T(8,128)(2,1)S(1)}, u32[]{:S(2)}, u32[]{:S(2)}) async-start(bf16[128,16,128]{2,0,1:T(8,128)(2,1)} %bitcast.132), calls=%async_computation | async-start | bytes 1048576 | tf_op jit(solution)/shard_map/all_to_all | solution.py:78
  23.9 18.3 %all-to-all-start.2 = ((bf16[128,16,128]{2,0,1:T(8,128)(2,1)}), bf16[128,16,128]{2,0,1:T(8,128)(2,1)S(1)}, u32[]{:S(2)}, u32[]{:S(2)}) async-start(bf16[128,16,128]{2,0,1:T(8,128)(2,1)} %bitcast.155), calls=%async_computation.2 | async-start | bytes 1048576 | tf_op jit(solution)/shard_map/all_to_all | solution.py:80
  42.2 18.4 %all-to-all-start.1 = ((bf16[128,16,128]{2,0,1:T(8,128)(2,1)}), bf16[128,16,128]{2,0,1:T(8,128)(2,1)}, u32[]{:S(2)}, u32[]{:S(2)}) async-start(bf16[128,16,128]{2,0,1:T(8,128)(2,1)} %bitcast.154), calls=%async_computation.1 | async-start | bytes 1048576 | tf_op jit(solution)/shard_map/all_to_all | solution.py:79
  48.2 13.8 %copy-start.6 = (s32[32,5]{0,1:T(8,128)}, s32[32,5]{0,1:T(8,128)S(1)}, u32[]{:S(2)}) copy-start(s32[32,5]{0,1:T(8,128)S(1)} %reduce-window.9) | copy-start | bytes 1924
  49.3 13.8 %copy-start.5 = (f32[128]{0:T(128)S(1)}, f32[128]{0:T(128)}, u32[]{:S(2)}) copy-start(f32[128]{0:T(128)} %param.24) | copy-start | bytes 1540
  49.3 13.8 %copy-start.13 = (f32[2]{0:T(128)S(1)}, f32[2]{0:T(128)}, u32[]{:S(2)}) copy-start(f32[2]{0:T(128)} %param.23) | copy-start | bytes 28
  51.8 11.3 %copy-start.2 = (bf16[2,512,2,2,64]{1,4,3,2,0:T(8,128)(2,1)S(1)}, bf16[2,512,2,2,64]{1,4,3,2,0:T(8,128)(2,1)}, u32[]{:S(2)}) copy-start(bf16[2,512,2,2,64]{1,4,3,2,0:T(8,128)(2,1)} %copy.57) | copy-start | bytes 1572868
  63.1 35.9 %slice-start = ((s32[32,5]{0,1:T(8,128)}), s32[32,4]{0,1:T(4,128)S(1)}, s32[]{:S(2)}) async-start(s32[32,5]{0,1:T(8,128)} %copy-done.6), calls=%async_computation.6 | async-start | bytes 4096 | tf_op jit(solution)/shard_map/slice.1
  72.0 4.0 %copy-start.3 = (bf16[1024,2,128]{0,2,1:T(8,128)(2,1)S(1)}, bf16[1024,2,128]{0,2,1:T(8,128)(2,1)}, u32[]{:S(2)}) copy-start(bf16[1024,2,128]{0,2,1:T(8,128)(2,1)} %get-tuple-element.204) | copy-start | bytes 1572868 | tf_op jit(solution)/shard_map/while
  86.8 4.0 %copy-start.3 = (bf16[1024,2,128]{0,2,1:T(8,128)(2,1)S(1)}, bf16[1024,2,128]{0,2,1:T(8,128)(2,1)}, u32[]{:S(2)}) copy-start(bf16[1024,2,128]{0,2,1:T(8,128)(2,1)} %get-tuple-element.204) | copy-start | bytes 1572868 | tf_op jit(solution)/shard_map/while
  95.1 18.2 %all-to-all-start.3 = ((bf16[1024,2,128]{2,1,0:T(2,128)(2,1)}), bf16[1024,2,128]{2,1,0:T(2,128)(2,1)S(1)}, u32[]{:S(2)}, u32[]{:S(2)}) async-start(bf16[1024,2,128]{2,1,0:T(2,128)(2,1)} %copy.59), calls=%async_computation.3 | async-start | bytes 1048576 | tf_op jit(solution)/shard_map/all_to_all | solution.py:83
  113.6 4.8 %copy-start.4 = (bf16[1,128,2048]{2,1,0:T(8,128)(2,1)S(1)}, bf16[1,128,2048]{2,1,0:T(8,128)(2,1)}, u32[]{:S(2)}) copy-start(bf16[1,128,2048]{2,1,0:T(8,128)(2,1)} %param.25) | copy-start | bytes 1572868
  113.6 4.8 %copy-start.7 = (f32[2048]{0:T(1024)S(1)}, f32[2048]{0:T(1024)}, u32[]{:S(2)}) copy-start(f32[2048]{0:T(1024)} %param.27) | copy-start | bytes 24580
  113.7 5.2 %copy-start.8 = (f32[2048]{0:T(1024)S(1)}, f32[2048]{0:T(1024)}, u32[]{:S(2)}) copy-start(f32[2048]{0:T(1024)} %param.28) | copy-start | bytes 24580
  125.5 76.3 %copy-start.12 = (bf16[1,2048,512]{2,1,0:T(8,128)(2,1)S(1)}, bf16[1,2048,512]{2,1,0:T(8,128)(2,1)}, u32[]{:S(2)}) copy-start(bf16[1,2048,512]{2,1,0:T(8,128)(2,1)} %param.32) | copy-start | bytes 6291460
  200.1 1.7 copy-start.1
  212.9 4.0 %copy-start.11 = (f32[1,128,4]{1,2,0:T(4,128)S(1)}, f32[1,128,4]{1,2,0:T(4,128)}, u32[]{:S(2)}) copy-start(f32[1,128,4]{1,2,0:T(4,128)} %param.31) | copy-start | bytes 6148
  212.9 75.3 %all-to-all-start.5 = ((bf16[32,24,2048]{2,1,0:T(8,128)(2,1)}), bf16[32,24,2048]{2,1,0:T(8,128)(2,1)}, u32[]{:S(2)}, u32[]{:S(2)}) async-start(bf16[32,24,2048]{2,1,0:T(8,128)(2,1)} %bitcast.149), calls=%async_computation.5 | async-start | bytes 6291456 | tf_op jit(solution)/shard_map/all_to_all | solution.py:121
  306.8 4.4 %copy-start.9 = (f32[2048]{0:T(1024)S(1)}, f32[2048]{0:T(1024)}, u32[]{:S(2)}) copy-start(f32[2048]{0:T(1024)} %param.29) | copy-start | bytes 24580
where the time goes:
time: 315 us; the launch traced here: 313 us
  waiting for transfers between devices  110 us (35%)
  blocking collectives  74.6 us (24%)
  local copies, waits for them, and re-layouts  44.7 us (14%)
  matrix products  38.3 us (12%)
  starting transfers between devices  22.7 us (7%)
  other arithmetic  21.5 us (7%)
    all_to_all x1, blocking collectives, local(): lax.all_to_all(outgoing, ('sp', 'dp'), split_axis=0, concat_axis=0, tiled...  74.6 us
    all_to_all x1, waiting for transfers between devices, local(): lax.all_to_all(results, ('sp', 'dp'), split_axis=0, concat_axis=0, tiled=...  69.1 us
    sub x2, matrix products, one_block(): exponent = jnp.exp(scores - maxima)  14.3 us
    all_to_all x1, waiting for transfers between devices, local(): lax.all_to_all(value_vectors[0], 'sp', split_axis=1, concat_axis=0, tiled...  12.7 us
    all_to_all x1, waiting for transfers between devices, local(): lax.all_to_all(queries[0], 'sp', split_axis=1, concat_axis=0, tiled=True)  12.5 us
    dot_general x2, matrix products, feed_forward(): jnp.dot(hidden, down_w, preferred_element_type=jnp.float32)  12.5 us
    unnamed x31, local copies, waits for them, and re-layouts  8.84 us
    div x2, other arithmetic, one_block(): softmax_both = exponent / jnp.sum(exponent, axis=-1, keepdims=True)  7.91 us
  transfers between devices with their start and end apart: 5, of which 5 were waited for; matrix products, arithmetic and copies ran while one was open for 6% of the time, Pallas kernels for 0%

commit v1 on v0

v1 whole, which is shorter than its diff:
```python
import jax
import jax.numpy as jnp
from jax import lax
from jax.experimental import pallas as pl
from jax.experimental.pallas import tpu as pltpu
from jax.sharding import PartitionSpec as P

epsilon = 1e-06


def rms_scale(values_in, gain):
    return (
        values_in
        * lax.rsqrt(jnp.mean(values_in * values_in, axis=-1, keepdims=True) + epsilon)
        * gain
    )


def feed_forward(rows, gate_w, up_w, down_w):
    gate_val = jnp.dot(rows, gate_w, preferred_element_type=jnp.float32)
    up_val = jnp.dot(rows, up_w, preferred_element_type=jnp.float32)
    hidden = (jax.nn.silu(gate_val) * up_val).astype(jnp.bfloat16)
    return jnp.dot(hidden, down_w, preferred_element_type=jnp.float32).astype(jnp.bfloat16)


def attend(packed, head_lambda, head_gain):
    length = packed.shape[0]
    head_count = head_lambda.shape[0]
    width = head_gain.shape[0]
    half = width // 2
    block = min(256, length)
    scale = half ** (-0.5)

    def body(lambda_ref, packed_ref, gain_ref, out_ref):
        lane = lax.broadcasted_iota(jnp.int32, (block, width), 1)
        row = lax.broadcasted_iota(jnp.int32, (block, block), 0)
        col = lax.broadcasted_iota(jnp.int32, (block, block), 1)
        causal = col <= row
        gain = gain_ref[...]
        contract = (((1,), (1,)), ((), ()))
        for head in range(head_count):
            q_col, k_col, v_col = (
                (part * head_count + head) * width for part in range(3)
            )
            for index in range(length // block):
                start = index * block
                query = packed_ref[start : start + block, q_col : q_col + width]
                query = query.astype(jnp.float32) * scale
                spans = ([(0, start)] if index else []) + [(start, start + block)]
                weights = []
                for part in range(2):
                    keep = (lane < half) if part == 0 else (lane >= half)
                    one = jnp.where(keep, query, 0.0).astype(jnp.bfloat16)
                    scores = [
                        lax.dot_general(
                            one,
                            packed_ref[low:high, k_col : k_col + width],
                            contract,
                            preferred_element_type=jnp.float32,
                        )
                        for low, high in spans
                    ]
                    scores[-1] = jnp.where(causal, scores[-1], -jnp.inf)
                    top = scores[0].max(axis=1, keepdims=True)
                    for other in scores[1:]:
                        top = jnp.maximum(top, other.max(axis=1, keepdims=True))
                    powers = [jnp.exp(s - top) for s in scores]
                    total = powers[0].sum(axis=1, keepdims=True)
                    for other in powers[1:]:
                        total = total + other.sum(axis=1, keepdims=True)
                    factor = 1.0 / total
                    if part == 1:
                        factor = factor * lambda_ref[head]
                    weights.append((powers, factor))
                result = None
                for place, (low, high) in enumerate(spans):
                    mixture = (
                        weights[0][0][place] * weights[0][1]
                        - weights[1][0][place] * weights[1][1]
                    ).astype(jnp.bfloat16)
                    piece = jnp.dot(
                        mixture,
                        packed_ref[low:high, v_col : v_col + width],
                        preferred_element_type=jnp.float32,
                    )
                    result = piece if result is None else result + piece
                out_ref[start : start + block, head * width : (head + 1) * width] = rms_scale(
                    result, gain
                ).astype(jnp.bfloat16)

    return pl.pallas_call(
        body,
        out_shape=jax.ShapeDtypeStruct((length, head_count * width), jnp.bfloat16),
        in_specs=[
            pl.BlockSpec(memory_space=pltpu.SMEM),
            pl.BlockSpec(memory_space=pltpu.VMEM),
            pl.BlockSpec(memory_space=pltpu.VMEM),
        ],
        out_specs=pl.BlockSpec(memory_space=pltpu.VMEM),
        compiler_params=pltpu.CompilerParams(vmem_limit_bytes=48 * 1024 * 1024),
        name="attend",
    )(head_lambda, packed, head_gain.reshape(1, width))


def finish(returned, high, low, shared_out, updated, post_gain):
    def body(ret_ref, high_ref, low_ref, shared_ref, updated_ref, gain_ref, out_ref):
        rows = ret_ref[...]
        combined = (
            jnp.dot(high_ref[...], rows, preferred_element_type=jnp.float32)
            + jnp.dot(low_ref[...], rows, preferred_element_type=jnp.float32)
            + shared_ref[...].astype(jnp.float32)
        )
        out_ref[...] = (
            updated_ref[...].astype(jnp.float32) + rms_scale(combined, gain_ref[...])
        ).astype(jnp.bfloat16)

    return pl.pallas_call(
        body,
        out_shape=jax.ShapeDtypeStruct(updated.shape, jnp.bfloat16),
        in_specs=[pl.BlockSpec(memory_space=pltpu.VMEM)] * 6,
        out_specs=pl.BlockSpec(memory_space=pltpu.VMEM),
        compiler_params=pltpu.CompilerParams(vmem_limit_bytes=48 * 1024 * 1024),
        name="finish",
    )(returned, high, low, shared_out, updated, post_gain.reshape(1, -1))


def slots_of(routes, experts_total, capacity):
    tok_count = routes.shape[0]
    expert_ids = jnp.arange(experts_total, dtype=jnp.int32)
    chosen = routes[:, :, None] == expert_ids[None, None, :]
    named = jnp.any(chosen, axis=1).astype(jnp.bfloat16)
    token_ids = jnp.arange(tok_count, dtype=jnp.int32)
    before = (token_ids[None, :] < token_ids[:, None]).astype(jnp.bfloat16)
    rank = jnp.dot(before, named, preferred_element_type=jnp.float32)
    own_rank = jnp.sum(jnp.where(chosen, rank[:, None, :], 0.0), axis=2).astype(jnp.int32)
    return routes * capacity + own_rank


def local(
    queries,
    key_vectors,
    value_vectors,
    head_lambda,
    head_gain,
    residual,
    out_weight,
    mix_gain,
    pre_gain,
    post_gain,
    routes,
    route_weights,
    expert_gate,
    expert_up,
    expert_down,
    shared_gate,
    shared_up,
    shared_down,
):
    sp_size = lax.axis_size("sp")
    tok_count, heads_total, width = queries.shape[1:]
    head_count = heads_total // sp_size
    packed = jnp.concatenate(
        [
            jnp.transpose(
                part[0].reshape(tok_count, sp_size, head_count * width), (1, 0, 2)
            )
            for part in (queries, key_vectors, value_vectors)
        ],
        axis=2,
    )
    packed = lax.all_to_all(packed, "sp", split_axis=0, concat_axis=0, tiled=True)
    attended = attend(
        packed.reshape(sp_size * tok_count, 3 * head_count * width), head_lambda, head_gain
    )
    token_heads = lax.all_to_all(
        attended.reshape(sp_size, tok_count, head_count * width),
        "sp",
        split_axis=0,
        concat_axis=0,
        tiled=True,
    )

    experts_total = sp_size * lax.axis_size("dp")
    top_count = routes.shape[2]
    capacity = 3 * tok_count * top_count // (2 * experts_total)
    slot_total = experts_total * capacity
    slots = slots_of(routes[0], experts_total, capacity)
    slot_ids = jnp.arange(slot_total, dtype=jnp.int32)
    pick = slots[:, :, None] == slot_ids[None, None, :]
    weight_rows = jnp.sum(jnp.where(pick, route_weights[0][:, :, None], 0.0), axis=1)
    high_part = lax.reduce_precision(weight_rows, 8, 7)
    high = high_part.astype(jnp.bfloat16)
    low = (weight_rows - high_part).astype(jnp.bfloat16)
    slots_t = slots.T
    place = (slots_t[0][None, :] == slot_ids[:, None]).astype(jnp.bfloat16)
    for k in range(1, top_count):
        place = place + (slots_t[k][None, :] == slot_ids[:, None]).astype(jnp.bfloat16)

    flat_heads = jnp.transpose(token_heads, (1, 0, 2)).reshape(tok_count, -1)
    mixed_rows = jnp.dot(flat_heads, out_weight, preferred_element_type=jnp.float32)
    updated = (residual[0].astype(jnp.float32) + rms_scale(mixed_rows, mix_gain)).astype(
        jnp.bfloat16
    )
    normed = rms_scale(updated.astype(jnp.float32), pre_gain).astype(jnp.bfloat16)
    model_width = normed.shape[1]
    outgoing = jnp.dot(place, normed, preferred_element_type=jnp.float32).astype(jnp.bfloat16)
    outgoing = outgoing.reshape(experts_total, capacity, model_width)
    arrived = lax.all_to_all(outgoing, ("sp", "dp"), split_axis=0, concat_axis=0, tiled=True)
    shared_out = feed_forward(normed, shared_gate, shared_up, shared_down)
    flat_rows = arrived.reshape(-1, model_width)
    result_rows = feed_forward(flat_rows, expert_gate[0], expert_up[0], expert_down[0])
    results = result_rows.reshape(arrived.shape[0], -1, model_width)
    returned = lax.all_to_all(results, ("sp", "dp"), split_axis=0, concat_axis=0, tiled=True)
    output = finish(
        returned.reshape(slot_total, model_width), high, low, shared_out, updated, post_gain
    )
    return output.reshape(1, tok_count, model_width)


def solution(mesh):
    in_specs = (
        P("dp", "sp", None, None),
        P("dp", "sp", None, None),
        P("dp", "sp", None, None),
        P("sp"),
        P(),
        P("dp", "sp", None),
        P(),
        P(),
        P(),
        P(),
        P("dp", "sp", None),
        P("dp", "sp", None),
        P(("sp", "dp"), None, None),
        P(("sp", "dp"), None, None),
        P(("sp", "dp"), None, None),
        P(),
        P(),
        P(),
    )
    out_specs = P("dp", "sp", None)
    return jax.shard_map(local, mesh=mesh, in_specs=in_specs, out_specs=out_specs, check_vma=False)
```

time: 315 us -> 248 us (0.79)
  blocking collectives: 74.6 us -> 119 us
  local copies, waits for them, and re-layouts: 44.7 us -> 8.96 us
  waiting for transfers between devices: 110 us -> 78.9 us
  other arithmetic: 21.5 us -> 0.83 us
  starting transfers between devices: 22.7 us -> 7.37 us
  matrix products: 38.3 us -> 23.1 us
  Pallas kernels: 0 us -> 9.46 us
    all_to_all x0 -> x1, blocking collectives: none -> 44.1 us  [local(): lax.all_to_all(packed, 'sp', split_axis=0, concat_axis=0, tiled=True)]
    all_to_all x4 -> x1, waiting for transfers between devices: 40.6 us -> 13.9 us  [local(): lax.all_to_all(attended.reshape(sp_size, tok_count, head_count * width),...]
    all_to_all x4 -> x1, starting transfers between devices: 18.7 us -> 3.6 us  [local(): lax.all_to_all(attended.reshape(sp_size, tok_count, head_count * width),...]
    sub x2 -> x0, matrix products: 14.3 us -> none  [one_block(): exponent = jnp.exp(scores - maxima)]
    gather x2 -> x0, local copies, waits for them, and re-layouts: 11.8 us -> none  [the longest x1 7.52 us: local(): picked = returned.reshape(experts_total * capacity, model_width)[slot_index]]
    pallas_call x0 -> x2, Pallas kernels: none -> 9.46 us  [the longest x1 5.54 us: attend(): pl.pallas_call(body, out_shape=jax.ShapeDtypeStruct((length, head_count *...]
    div x2 -> x0, other arithmetic: 7.91 us -> none  [one_block(): softmax_both = exponent / jnp.sum(exponent, axis=-1, keepdims=True)]
    unnamed x31 -> x24, local copies, waits for them, and re-layouts: 8.84 us -> 1.99 us
  transfers between devices with their start and end apart: 5 -> 2, of which waited for: 5 -> 2; matrix products, arithmetic and copies ran while one was open for 6% -> 3% of each run, Pallas kernels for 0% -> 0%
where the time goes in v1:
time: 248 us
  blocking collectives  119 us (48%)
  waiting for transfers between devices  78.9 us (32%)
  matrix products  23.1 us (9%)
  Pallas kernels  9.46 us (4%)
  local copies, waits for them, and re-layouts  8.96 us (4%)
  starting transfers between devices  7.37 us (3%)
    all_to_all x1, blocking collectives, local(): lax.all_to_all(outgoing, ('sp', 'dp'), split_axis=0, concat_axis=0, tiled...  74.6 us
    all_to_all x1, waiting for transfers between devices, local(): lax.all_to_all(results, ('sp', 'dp'), split_axis=0, concat_axis=0, tiled=...  65 us
    all_to_all x1, blocking collectives, local(): lax.all_to_all(packed, 'sp', split_axis=0, concat_axis=0, tiled=True)  44.1 us
    all_to_all x1, waiting for transfers between devices, local(): lax.all_to_all(attended.reshape(sp_size, tok_count, head_count * width),...  13.9 us
    dot_general x2, matrix products, feed_forward(): jnp.dot(hidden, down_w, preferred_element_type=jnp.float32)  11.3 us
    dot_general x2, matrix products, feed_forward(): gate_val = jnp.dot(rows, gate_w, preferred_element_type=jnp.float32)  5.74 us
    pallas_call x1, Pallas kernels, attend(): pl.pallas_call(body, out_shape=jax.ShapeDtypeStruct((length, head_count *...  5.54 us
  transfers between devices with their start and end apart: 2, of which 2 were waited for; matrix products, arithmetic and copies ran while one was open for 3% of the time, Pallas kernels for 0%

profile of v1, /device:TPU:0, one launch (start us, length us, event | category | flops | bytes accessed | tf_op | source)
XLA Modules:
  0.0 247.5 jit_solution(12049063439479416072)
XLA Ops:
  0.0 1.4 reshape_squeeze.10
  1.4 2.0 reshape_squeeze.11
  3.4 1.2 reshape_squeeze.9
  4.7 1.3 copy_bitcast_fusion
  6.1 44.1 %all_to_all.20 = bf16[8,128,768]{2,1,0:T(8,128)(2,1)S(1)} all-to-all(bf16[8,128,768]{2,1,0:T(8,128)(2,1)S(1)} %pad_maximum_fusion), channel_id=1, replica_groups=mesh['sp'=8,'dp'=4] {'sp'}, dimensions={0} | all-to-all | bytes 3145728 | tf_op jit(solution)/shard_map/all_to_all | solution.py:171
  50.2 5.5 %attend.1 = bf16[1024,256]{1,0:T(8,128)(2,1)S(1)} custom-call(f32[2]{0:T(128)S(1)} %copy-done.2, bf16[1024,768]{1,0:T(8,128)(2,1)S(1)} %bitcast.62, f32[1,128]{1,0:T(1,128)S(1)} %bitcast.65), custom_call_target="tpu_custom_call" | custom-call | tf_op jit(solution)/shard_map/attend/pallas_call | solution.py:91
  55.8 1.0 copy.37
  56.8 3.6 %all-to-all-start.1 = ((bf16[8,128,256]{1,2,0:T(8,128)(2,1)}), bf16[8,128,256]{1,2,0:T(8,128)(2,1)S(1)}, u32[]{:S(2)}, u32[]{:S(2)}) async-start(bf16[8,128,256]{1,2,0:T(8,128)(2,1)} %copy.37), calls=%async_computation.1 | async-start | bytes 1048576 | tf_op jit(solution)/shard_map/all_to_all | solution.py:175
  60.4 0.1 fusion.37
  60.6 13.9 %all-to-all-done.1 = bf16[8,128,256]{1,2,0:T(8,128)(2,1)S(1)} async-done(((bf16[8,128,256]{1,2,0:T(8,128)(2,1)}), bf16[8,128,256]{1,2,0:T(8,128)(2,1)S(1)}, u32[]{:S(2)}, u32[]{:S(2)}) %all-to-all-start.1) | async-done | bytes 524320 | tf_op jit(solution)/shard_map/all_to_all | solution.py:175
  74.6 4.8 %multiply_reduce_fusion = (f32[128]{0:T(128)S(1)}, f32[128,2048]{1,0:T(8,128)S(1)}) fusion(bf16[128,2048]{0,1:T(8,128)(2,1)S(1)} %bitcast.67, bf16[2048,2048]{1,0:T(8,128)(2,1)} %param.24), kind=kOutput, calls=%fused_computation.21 | convolution fusion | flops 1074265984 | bytes 9961984 | tf_op jit(solution)/shard_map/dot_general | solution.py:200
  79.4 0.4 fusion.8
  79.8 0.3 copy-done.6
  80.1 1.1 convolution_convert_fusion.1
  81.1 74.6 %all_to_all.21 = bf16[32,24,2048]{2,1,0:T(8,128)(2,1)S(1)} all-to-all(bf16[32,24,2048]{2,1,0:T(8,128)(2,1)S(1)} %bitcast.66), channel_id=1, replica_groups=mesh['sp'=8,'dp'=4] {'sp','dp'}, dimensions={0} | all-to-all | bytes 6291456 | tf_op jit(solution)/shard_map/all_to_all | solution.py:208
  155.8 1.7 copy-done.4
  157.4 2.9 %fusion.3 = f32[768,512]{1,0:T(8,128)} fusion(bf16[768,2048]{1,0:T(8,128)(2,1)S(1)} %bitcast.69, bf16[1,2048,512]{2,1,0:T(8,128)(2,1)S(1)} %copy-done.11), kind=kOutput, calls=%fused_computation.6 | convolution fusion | flops 1610612736 | bytes 6815744 | tf_op jit(solution)/shard_map/dot_general | solution.py:20
  160.4 8.1 %convolution_convert_fusion = bf16[768,2048]{1,0:T(8,128)(2,1)} fusion(bf16[1,512,2048]{2,1,0:T(8,128)(2,1)S(1)} %copy-done, f32[768,512]{1,0:T(8,128)} %fusion.3, bf16[768,2048]{1,0:T(8,128)(2,1)} %bitcast.70, bf16[1,2048,512]{2,1,0:T(8,128)(2,1)} %param.31), kind=kOutput, calls=%fused_computation | convolution fusion | flops 3225157632 | bytes 12058624 | tf_op jit(solution)/shard_map/dot_general | solution.py:23
  168.5 3.8 %all-to-all-start.3 = ((bf16[32,24,2048]{2,1,0:T(8,128)(2,1)}), bf16[32,24,2048]{2,1,0:T(8,128)(2,1)}, u32[]{:S(2)}, u32[]{:S(2)}) async-start(bf16[32,24,2048]{2,1,0:T(8,128)(2,1)} %bitcast.68), calls=%async_computation.3 | async-start | bytes 6291456 | tf_op jit(solution)/shard_map/all_to_all | solution.py:213
  172.3 0.2 select_reduce_fusion
  172.6 2.8 %fusion.42 = f32[128,512]{1,0:T(8,128)} fusion(bf16[2048,512]{1,0:T(8,128)(2,1)} %param.33, bf16[128,2048]{1,0:T(8,128)(2,1)S(1)} %get-tuple-element.6.updated_ref, f32[2048]{0:T(1024)S(1)} %copy-done.6, f32[128]{0:T(128)S(1)} %add_rsqrt_fusion), kind=kOutput, calls=%fused_computation.63 | convolution fusion | flops 269484032 | bytes 2892288 | tf_op jit(solution)/shard_map/dot_general | solution.py:20
  175.4 3.2 %convolution_convert_fusion.2.shared_ref = bf16[128,2048]{1,0:T(8,128)(2,1)S(1)} fusion(bf16[512,2048]{1,0:T(8,128)(2,1)} %param.35, bf16[2048,512]{1,0:T(8,128)(2,1)} %param.34, f32[128,512]{1,0:T(8,128)} %fusion.42, bf16[128,2048]{1,0:T(8,128)(2,1)S(1)} %get-tuple-element.6.updated_ref, f32[2048]{0:T(1024)S(1)} %copy-done.6, f32[128]{0:T(128)} %copy-done.10), kind=kOutput, calls=%fused_computation.2 | convolution fusion | flops 538574848 | bytes 5513728 | tf_op jit(solution)/shard_map/dot_general | solution.py:23
  178.6 65.0 %all-to-all-done.3 = bf16[32,24,2048]{2,1,0:T(8,128)(2,1)} async-done(((bf16[32,24,2048]{2,1,0:T(8,128)(2,1)}), bf16[32,24,2048]{2,1,0:T(8,128)(2,1)}, u32[]{:S(2)}, u32[]{:S(2)}) %all-to-all-start.3) | async-done | bytes 3145760 | tf_op jit(solution)/shard_map/all_to_all | solution.py:213
  243.6 3.9 %finish.1 = bf16[128,2048]{1,0:T(8,128)(2,1)} custom-call(bf16[768,2048]{1,0:T(8,128)(2,1)} %bitcast.21.ret_ref, bf16[128,768]{1,0:T(8,128)(2,1)S(1)} %get-tuple-element.8.high_ref, bf16[128,768]{1,0:T(8,128)(2,1)S(1)} %get-tuple-element.7.low_ref, bf16[128,2048]{1,0:T(8,128)(2,1)S(1)} %convolution_convert_fusion.2.shared_ref, ...), custom_call_target="tpu_custom_call" | custom-call | tf_op jit(solution)/shard_map/finish/pallas_call | solution.py:117
  (31 shorter events, 0.4 us)
Async XLA Ops:
  0.0 160.4 %copy-start = (bf16[1,512,2048]{2,1,0:T(8,128)(2,1)S(1)}, bf16[1,512,2048]{2,1,0:T(8,128)(2,1)}, u32[]{:S(2)}) copy-start(bf16[1,512,2048]{2,1,0:T(8,128)(2,1)} %param.32) | copy-start | bytes 6291460
  6.1 44.1 %copy-start.2 = (f32[2]{0:T(128)S(1)}, f32[2]{0:T(128)}, u32[]{:S(2)}) copy-start(f32[2]{0:T(128)} %lambda_ref.1) | copy-start | bytes 28
  6.1 44.1 %copy-start.3 = (f32[128]{0:T(128)S(1)}, f32[128]{0:T(128)}, u32[]{:S(2)}) copy-start(f32[128]{0:T(128)} %param.22) | copy-start | bytes 1540
  50.2 10.2 %copy-start.7 = (s32[1,128,4]{1,2,0:T(4,128)S(1)}, s32[1,128,4]{1,2,0:T(4,128)}, u32[]{:S(2)}) copy-start(s32[1,128,4]{1,2,0:T(4,128)} %param.28) | copy-start | bytes 6148
  56.8 17.8 %all-to-all-start.1 = ((bf16[8,128,256]{1,2,0:T(8,128)(2,1)}), bf16[8,128,256]{1,2,0:T(8,128)(2,1)S(1)}, u32[]{:S(2)}, u32[]{:S(2)}) async-start(bf16[8,128,256]{1,2,0:T(8,128)(2,1)} %copy.37), calls=%async_computation.1 | async-start | bytes 1048576 | tf_op jit(solution)/shard_map/all_to_all | solution.py:175
  74.6 4.8 %copy-start.5 = (bf16[1,128,2048]{2,1,0:T(8,128)(2,1)S(1)}, bf16[1,128,2048]{2,1,0:T(8,128)(2,1)}, u32[]{:S(2)}) copy-start(bf16[1,128,2048]{2,1,0:T(8,128)(2,1)} %param.23) | copy-start | bytes 1572868
  74.6 4.8 %copy-start.8 = (f32[2048]{0:T(1024)S(1)}, f32[2048]{0:T(1024)}, u32[]{:S(2)}) copy-start(f32[2048]{0:T(1024)} %param.25) | copy-start | bytes 24580
  79.4 0.7 copy-start.6
  79.8 92.8 %copy-start.10 = (f32[128]{0:T(128)}, f32[128]{0:T(128)S(1)}, u32[]{:S(2)}) copy-start(f32[128]{0:T(128)S(1)} %add_rsqrt_fusion) | copy-start | bytes 1540
  81.1 76.3 %copy-start.11 = (bf16[1,2048,512]{2,1,0:T(8,128)(2,1)S(1)}, bf16[1,2048,512]{2,1,0:T(8,128)(2,1)}, u32[]{:S(2)}) copy-start(bf16[1,2048,512]{2,1,0:T(8,128)(2,1)} %param.30) | copy-start | bytes 6291460
  155.8 1.7 copy-start.4
  168.5 3.8 %copy-start.9 = (f32[1,128,4]{1,2,0:T(4,128)S(1)}, f32[1,128,4]{1,2,0:T(4,128)}, u32[]{:S(2)}) copy-start(f32[1,128,4]{1,2,0:T(4,128)} %param.29) | copy-start | bytes 6148
  168.5 75.1 %all-to-all-start.3 = ((bf16[32,24,2048]{2,1,0:T(8,128)(2,1)}), bf16[32,24,2048]{2,1,0:T(8,128)(2,1)}, u32[]{:S(2)}, u32[]{:S(2)}) async-start(bf16[32,24,2048]{2,1,0:T(8,128)(2,1)} %bitcast.68), calls=%async_computation.3 | async-start | bytes 6291456 | tf_op jit(solution)/shard_map/all_to_all | solution.py:213
  175.4 68.2 %copy-start.1 = (f32[2048]{0:T(1024)S(1)}, f32[2048]{0:T(1024)}, u32[]{:S(2)}) copy-start(f32[2048]{0:T(1024)} %param.27) | copy-start | bytes 24580
